TPU v7x, 128 devices: a whole 4x4x4 slice. The times are simulated.
128 devices in a mesh: fs: 16 (over z, y), tp: 8 (over x, core).
Axes of the slice: x: 4, y: 4, z: 4, core: 2. Of those that a mesh axis runs over, the one named last changes fastest.
Arguments:
- fresh_rows: bfloat16 [16384, 2048], P('fs'), may hold values from -6 to 6
- saved_rows: bfloat16 [16384, 2048], P('fs'), may hold values from -6 to 6
- upstream_grad: bfloat16 [16384, 2048], P('fs'), may hold values from -6 to 6
- proj_up: bfloat16 [2048, 8192], P('fs', 'tp'), may hold values from -0.125 to 0.125
- proj_down: bfloat16 [2048, 8192], P('fs', 'tp'), may hold values from -0.0625 to 0.0625
- accum_up: float32 [2048, 8192], P('fs', 'tp'), may hold values from -6 to 6
- accum_down: float32 [2048, 8192], P('fs', 'tp'), may hold values from -6 to 6
Outputs:
- fresh_out: bfloat16 [16384, 2048], P(('fs', 'tp'))
- saved_grad: bfloat16 [16384, 2048], P(('fs', 'tp'))
- accum_up_out: float32 [2048, 8192], P('fs', 'tp')
- accum_down_out: float32 [2048, 8192], P('fs', 'tp')
All inputs are finite; a program needn't handle non-finite values.
Results may differ from a plain program's by a relative error of at most 0.014.
Values may be sent and summed in bfloat16 or wider, within the bound.
A program may use at most 128 MiB of HBM per device.

v0:
```python
import jax
import jax.numpy as jnp
from jax import lax
from jax.sharding import PartitionSpec as P


def side_by_side(arrays, axis, dim, along):
    both = jnp.concatenate(arrays, axis=along)
    filled, at, gathered = (lax.all_gather(both, axis, axis=dim, tiled=True), 0, [])
    for a in arrays:
        gathered.append(lax.slice_in_dim(filled, at, at + a.shape[along], axis=along))
        at += a.shape[along]
    return tuple(gathered)


def split_up(array, dim, count):
    lengths = array.shape
    blocks = array.reshape(*lengths[:dim], count, lengths[dim] // count, *lengths[dim + 1 :])
    return jnp.moveaxis(blocks, dim, 0)


def sum_at_owner(array, axis, dim):
    count = lax.axis_size(axis)
    blocks = lax.all_to_all(split_up(array, dim, count), axis, 0, 0, tiled=True)
    return jnp.sum(blocks.astype(jnp.float32), axis=0)


def against_rows(left, right):
    return lax.dot_general(
        left, right, (((1,), (1,)), ((), ())), preferred_element_type=jnp.float32
    )


def over_tokens(left, right):
    return lax.dot_general(
        left, right, (((0,), (0,)), ((), ())), preferred_element_type=jnp.float32
    )


def squared_relu(pre_values):
    active = jnp.maximum(pre_values, 0.0)
    return (active, (active * active).astype(jnp.bfloat16))


def body(fresh_rows, saved_rows, upstream_grad, proj_up, proj_down, accum_up, accum_down):
    row_count = fresh_rows.shape[0]
    grad_scale = float(row_count * lax.axis_size("fs")) ** (-0.5)
    up_whole, down_whole = side_by_side((proj_up, proj_down), "fs", 0, 1)
    fresh_pre = jnp.dot(fresh_rows, up_whole, preferred_element_type=jnp.float32)
    fresh_active, fresh_hidden = squared_relu(fresh_pre)
    fresh_term = against_rows(fresh_hidden, down_whole)
    up_back, down_back = (up_whole, down_whole)
    saved_pre = jnp.dot(saved_rows, up_back, preferred_element_type=jnp.float32)
    saved_active, saved_hidden = squared_relu(saved_pre)
    down_sum = lax.psum_scatter(
        (grad_scale * over_tokens(upstream_grad, saved_hidden)).astype(jnp.bfloat16),
        "fs",
        scatter_dimension=0,
        tiled=True,
    ).astype(jnp.float32)
    hidden_grad = jnp.dot(upstream_grad, down_back, preferred_element_type=jnp.float32)
    pre_grad = (2.0 * saved_active * hidden_grad).astype(jnp.bfloat16)
    input_part = against_rows(pre_grad, up_back)
    mixed = sum_at_owner(jnp.stack((fresh_term, input_part), axis=1).astype(jnp.bfloat16), "tp", 0)
    fresh_out = mixed[:, 0, :].astype(jnp.bfloat16)
    saved_grad = mixed[:, 1, :].astype(jnp.bfloat16)
    up_sum = lax.psum_scatter(
        (grad_scale * over_tokens(saved_rows, pre_grad)).astype(jnp.bfloat16),
        "fs",
        scatter_dimension=0,
        tiled=True,
    ).astype(jnp.float32)
    accum_up_out = accum_up + up_sum
    accum_down_out = accum_down + down_sum
    return (fresh_out, saved_grad, accum_up_out, accum_down_out)


def solution(mesh):
    in_specs = (
        P("fs", None),
        P("fs", None),
        P("fs", None),
        P("fs", "tp"),
        P("fs", "tp"),
        P("fs", "tp"),
        P("fs", "tp"),
    )
    out_specs = (P(("fs", "tp"), None), P(("fs", "tp"), None), P("fs", "tp"), P("fs", "tp"))
    return jax.shard_map(body, mesh=mesh, in_specs=in_specs, out_specs=out_specs, check_vma=False)
```

profile of v0, /device:TPU:1, one launch (start us, length us, event | category | flops | bytes accessed | tf_op | source)
XLA Modules:
  0.0 276.6 jit_solution(16612528226734664391)
XLA Ops:
  7.2 0.0 all-gather.2.cloned.1.call-start
  7.2 1.9 pad_maximum_fusion.1
  9.1 0.0 all-gather.2.cloned.1.call-update
  9.1 0.0 reduce-scatter.9.cloned.1.call-start
  9.1 75.5 %all-gather.2.cloned.1.call-done = bf16[2048,2048]{1,0:T(8,128)(2,1)} async-done(((bf16[128,2048]{1,0:T(8,128)(2,1)}), bf16[2048,2048]{1,0:T(8,128)(2,1)}) %all-gather.2.cloned.1.call-update) | async-done | bytes 8388624 | tf_op jit(solution)/shard_map/all_gather | solution.py:9
  84.7 0.0 copy-start.2
  84.7 7.8 %fusion.6 = f32[1024,1024]{1,0:T(8,128)S(1)} fusion(bf16[1024,2048]{1,0:T(8,128)(2,1)} %param.8, bf16[2048,2048]{1,0:T(8,128)(2,1)} %all-gather.2.cloned.1.call-done), kind=kOutput, calls=%fused_computation.14 | convolution fusion | flops 4294967296 | bytes 12582912 | tf_op jit(solution)/shard_map/dot_general | solution.py:53
  92.5 0.0 copy-start.4
  92.5 1.9 copy-done.4
  94.4 0.0 copy-done.2
  94.4 6.0 %fusion.4 = bf16[2048,1024]{0,1:T(8,128)(2,1)} fusion(bf16[1024,2048]{1,0:T(8,128)(2,1)S(1)} %copy-done.2, f32[1024,1024]{1,0:T(8,128)S(1)} %fusion.6), kind=kOutput, calls=%fused_computation.12 | convolution fusion | flops 4302307328 | bytes 12582912 | tf_op jit(solution)/shard_map/dot_general | solution.py:35
  100.5 6.4 %copy.23 = bf16[2048,1024]{1,0:T(8,128)(2,1)} copy(bf16[2048,1024]{0,1:T(8,128)(2,1)} %fusion.4) | data formatting | bytes 8388608
  106.9 0.0 reduce-scatter.9.cloned.1.call-update
  106.9 0.0 reduce-scatter.7.cloned.1.call-start
  106.9 0.0 copy-start.3
  106.9 9.3 %multiply_convert_fusion.3 = bf16[1024,1024]{1,0:T(8,128)(2,1)S(1)} fusion(f32[1024,1024]{1,0:T(8,128)} %copy-done.4, bf16[1024,2048]{1,0:T(8,128)(2,1)} %param.9, bf16[2048,2048]{1,0:T(8,128)(2,1)} %all-gather.2.cloned.1.call-done), kind=kOutput, calls=%fused_computation.4 | convolution fusion | flops 4299161600 | bytes 14680064 | tf_op jit(solution)/shard_map/dot_general | solution.py:61
  116.3 0.0 copy-done.3
  116.3 6.3 %fusion.3 = bf16[2048,1024]{0,1:T(8,128)(2,1)} fusion(bf16[1024,1024]{1,0:T(8,128)(2,1)S(1)} %multiply_convert_fusion.3, bf16[1024,2048]{1,0:T(8,128)(2,1)S(1)} %copy-done.3), kind=kOutput, calls=%fused_computation.11 | convolution fusion | flops 4299161600 | bytes 10485760 | tf_op jit(solution)/shard_map/dot_general | solution.py:35
  122.6 6.5 %copy.21 = bf16[2048,1024]{1,0:T(8,128)(2,1)} copy(bf16[2048,1024]{0,1:T(8,128)(2,1)} %fusion.3) | data formatting | bytes 8388608
  129.1 0.0 reduce-scatter.7.cloned.1.call-update
  129.1 8.4 %convolution_convert_fusion = bf16[1024,2048]{1,0:T(8,128)(2,1)} fusion(bf16[1024,1024]{1,0:T(8,128)(2,1)S(1)} %multiply_convert_fusion.3, bf16[2048,2048]{1,0:T(8,128)(2,1)} %all-gather.2.cloned.1.call-done), kind=kOutput, calls=%fused_computation.6 | convolution fusion | flops 4297064448 | bytes 10485760 | tf_op jit(solution)/shard_map/dot_general | solution.py:29
  137.5 14.7 %convolution_convert_fusion.1 = bf16[1024,2048]{1,0:T(8,128)(2,1)} fusion(bf16[2048,2048]{1,0:T(8,128)(2,1)} %all-gather.2.cloned.1.call-done, bf16[1024,2048]{1,0:T(8,128)(2,1)} %param.7), kind=kOutput, calls=%fused_computation.7 | convolution fusion | flops 8595177472 | bytes 16777216 | tf_op jit(solution)/shard_map/dot_general | solution.py:29
  152.1 7.6 %pad_maximum_fusion = bf16[8,128,2,2048]{3,1,2,0:T(8,128)(2,1)} fusion(bf16[8,128,1,2048]{3,1,2,0:T(8,128)(2,1)} %bitcast.23, bf16[8,128,1,2048]{3,1,2,0:T(8,128)(2,1)} %bitcast.24), kind=kLoop, calls=%fused_computation | loop fusion | flops 4194304 | bytes 16777216 | tf_op jit(solution)/shard_map/stack | solution.py:64
  159.7 0.0 copy-start
  159.7 0.0 copy-start.1
  159.7 5.9 %all-to-all-start = ((bf16[8,128,2,2048]{3,1,2,0:T(8,128)(2,1)}), bf16[8,128,2,2048]{3,1,2,0:T(8,128)(2,1)}, u32[]{:S(2)}, u32[]{:S(2)}) async-start(bf16[8,128,2,2048]{3,1,2,0:T(8,128)(2,1)} %pad_maximum_fusion), calls=%async_computation | async-start | bytes 16777216 | tf_op jit(solution)/shard_map/all_to_all | solution.py:24
  165.6 0.0 copy-done
  165.6 0.2 copy.17
  165.8 0.0 copy-done.1
  165.8 0.2 copy.18
  166.0 93.3 %all-to-all-done = bf16[8,128,2,2048]{3,1,2,0:T(8,128)(2,1)} async-done(((bf16[8,128,2,2048]{3,1,2,0:T(8,128)(2,1)}), bf16[8,128,2,2048]{3,1,2,0:T(8,128)(2,1)}, u32[]{:S(2)}, u32[]{:S(2)}) %all-to-all-start) | async-done | bytes 8388640 | tf_op jit(solution)/shard_map/all_to_all | solution.py:24
  259.4 5.3 %reduce = bf16[128,2,2048]{2,0,1:T(8,128)(2,1)S(1)} reduce(bf16[8,128,2,2048]{3,1,2,0:T(8,128)(2,1)} %all-to-all-done, bf16[]{:T(256)} %constant.2), dimensions={0}, to_apply=%region_0.0.clone | reduce | flops 3670016 | bytes 9437186 | tf_op jit(solution)/shard_map/reduce_sum | solution.py:25
  264.7 1.0 slice_bitcast_fusion
  265.7 0.0 reduce-scatter.9.cloned.1.call-done
  265.7 1.1 copy.24
  266.9 1.0 copy.20
  267.9 0.0 reduce-scatter.7.cloned.1.call-done
  267.9 1.1 copy.22
  269.1 1.0 copy.19
  (2 shorter events, 0.1 us)
Async XLA Ops:
  7.2 77.5 %all-gather.2.cloned.1.call-start = ((), (), s32[]{:S(2)}) async-start(), calls=%async_computation.3 | async-start | bytes 8912896 | tf_op jit(solution)/shard_map/all_gather | solution.py:9
  9.1 256.6 %reduce-scatter.9.cloned.1.call-start = ((), (), s32[]{:S(2)}) async-start(), calls=%async_computation.5 | async-start | bytes 4456448
  84.7 9.7 %copy-start.2 = (bf16[1024,2048]{1,0:T(8,128)(2,1)S(1)}, bf16[1024,2048]{1,0:T(8,128)(2,1)}, u32[]{:S(2)}) copy-start(bf16[1024,2048]{1,0:T(8,128)(2,1)} %param.9) | copy-start | bytes 12582916
  92.5 2.0 copy-start.4
  106.9 161.0 %reduce-scatter.7.cloned.1.call-start = ((), (), s32[]{:S(2)}) async-start(), calls=%async_computation.4 | async-start | bytes 4456448
  106.9 9.4 %copy-start.3 = (bf16[1024,2048]{1,0:T(8,128)(2,1)S(1)}, bf16[1024,2048]{1,0:T(8,128)(2,1)}, u32[]{:S(2)}) copy-start(bf16[1024,2048]{1,0:T(8,128)(2,1)} %param.8) | copy-start | bytes 12582916
  159.7 5.9 %copy-start = (f32[128,1024]{1,0:T(8,128)S(1)}, f32[128,1024]{1,0:T(8,128)}, u32[]{:S(2)}) copy-start(f32[128,1024]{1,0:T(8,128)} %param.12) | copy-start | bytes 1572868
  159.7 6.1 %copy-start.1 = (f32[128,1024]{1,0:T(8,128)S(1)}, f32[128,1024]{1,0:T(8,128)}, u32[]{:S(2)}) copy-start(f32[128,1024]{1,0:T(8,128)} %param.13) | copy-start | bytes 1572868
  159.7 99.7 %all-to-all-start = ((bf16[8,128,2,2048]{3,1,2,0:T(8,128)(2,1)}), bf16[8,128,2,2048]{3,1,2,0:T(8,128)(2,1)}, u32[]{:S(2)}, u32[]{:S(2)}) async-start(bf16[8,128,2,2048]{3,1,2,0:T(8,128)(2,1)} %pad_maximum_fusion), calls=%async_computation | async-start | bytes 16777216 | tf_op jit(solution)/shard_map/all_to_all | solution.py:24
Sparse Core Ops, SparseCore 0:
  10.7 73.9 all-gather.1
  107.0 76.8 reduce-scatter.8
  187.2 77.8 reduce-scatter.6
where the time goes:
time: 277 us
  waiting for transfers between devices  169 us (61%)
  matrix products  52.5 us (19%)
  local copies, waits for them, and re-layouts  20.5 us (7%)
  other arithmetic  14.8 us (5%)
  between operations  13.9 us (5%)
  starting transfers between devices  6.06 us (2%)
    all_to_all x1, waiting for transfers between devices, sum_at_owner(): blocks = lax.all_to_all(split_up(array, dim, count), axis, 0, 0, tiled=True)  93.3 us
    all_gather x1, waiting for transfers between devices, side_by_side(): lax.all_gather(both, axis, axis=dim, tiled=True)  75.5 us
    dot_general x2, matrix products, against_rows(): lax.dot_general(left, right, (((1,), (1,)), ((), ())), preferred_element_...  23 us
    unnamed x18, local copies, waits for them, and re-layouts  19.4 us
    dot_general x2, matrix products, over_tokens(): lax.dot_general(left, right, (((0,), (0,)), ((), ())), preferred_element_...  12.3 us
    dot_general x1, matrix products, body(): jnp.dot(upstream_grad, down_back, preferred_element_type=jnp.float32)  9.33 us
    dot_general x1, matrix products, body(): saved_pre = jnp.dot(saved_rows, up_back, preferred_element_type=jnp.float32)  7.76 us
    another operation x1, other arithmetic, body(): jnp.stack((fresh_term, input_part), axis=1).astype(jnp.bfloat16)  7.56 us
  transfers between devices with their start and end apart: 4, of which 2 were waited for; matrix products, arithmetic and copies ran while one was open for 22% of the time, Pallas kernels for 0%

commit v1 on v0

v1 whole, which is shorter than its diff:
```python
import jax
import jax.numpy as jnp
from jax import lax
from jax.experimental import pallas as pl
from jax.experimental.pallas import tpu as pltpu
from jax.sharding import PartitionSpec as P

MESH = pl.DeviceIdType.MESH
BF = jnp.bfloat16
F32 = jnp.float32
COLS = (slice(0, 512), slice(512, 1024))
N_GATHER = 48
N_GRADS = 48
N_X = 20
N_MSG = N_GATHER + N_GRADS + N_X


def rows_at(start, size):
    return pl.ds(pl.multiple_of(start, size), size)


def kernel(
    fresh_hbm, saved_hbm, upstream_hbm, up_hbm, down_hbm, accum_up_hbm, accum_down_hbm,
    fresh_out, saved_grad, accum_up_out, accum_down_out,
    fresh, saved, upstream, up_w, down_w, accum_up, accum_down,
    fresh_hidden, saved_active, saved_hidden, pre_grad, grad_down, grad_up,
    land_z, land_y, land_2, land_pair, land_x,
    send_sem, recv_sem, load_sem,
):
    fs, tp = lax.axis_index("fs"), lax.axis_index("tp")
    z, y, x, core = fs // 4, fs % 4, tp // 2, tp % 2

    def nxt(p, by):
        return lax.rem(p + by, 4)

    to = {
        ("y", 1): (z * 4 + nxt(y, 1), tp),
        ("y", -1): (z * 4 + nxt(y, 3), tp),
        ("z", 1): (nxt(z, 1) * 4 + y, tp),
        ("z", -1): (nxt(z, 3) * 4 + y, tp),
        ("x", 1): (fs, nxt(x, 1) * 2 + core),
        ("x", -1): (fs, nxt(x, 3) * 2 + core),
        "pair": (fs, x * 2 + 1 - core),
    }
    place = {"y": y, "z": z, "x": x}
    used = [0]
    sent = []

    def reserve(count):
        used[0] += count
        return used[0] - count

    def message(src, dst, index, target):
        return pltpu.make_async_remote_copy(
            src_ref=src,
            dst_ref=dst,
            send_sem=send_sem.at[index],
            recv_sem=recv_sem.at[index],
            device_id=target,
            device_id_type=MESH,
        )

    def send(src, dst, index, target):
        copy = message(src, dst, index, target)
        copy.start()
        sent.append(copy)

    def arrived(dst, index, target):
        message(dst, dst, index, target).wait_recv()

    class Gather:
        def __init__(self, axis, block):
            self.plus, self.minus = to[(axis, 1)], to[(axis, -1)]
            p = place[axis]
            self.block = block
            self.here, self.after, self.across, self.before = p, nxt(p, 1), nxt(p, 2), nxt(p, 3)
            self.base = reserve(6)

        def go(self, half, index, owner, target):
            part = self.block(owner, half)
            send(part, part, self.base + index, target)

        def got(self, half, index, owner, target):
            arrived(self.block(owner, half), self.base + index, target)

        def start(self):
            self.go(0, 0, self.here, self.plus)
            self.go(1, 2, self.here, self.minus)
            self.go(1, 1, self.here, self.plus)
            self.go(0, 3, self.here, self.minus)

        def mid(self):
            self.got(0, 0, self.before, self.plus)
            self.go(0, 4, self.before, self.plus)
            self.got(1, 2, self.after, self.minus)
            self.go(1, 5, self.after, self.minus)

        def end(self):
            self.got(1, 1, self.before, self.plus)
            self.got(0, 3, self.after, self.minus)
            self.got(0, 4, self.across, self.plus)
            self.got(1, 5, self.across, self.minus)

    class Scatter:
        def __init__(self, axis, block, land):
            self.plus, self.minus = to[(axis, 1)], to[(axis, -1)]
            p = place[axis]
            self.block, self.land = block, land
            self.here, self.after, self.across, self.before = p, nxt(p, 1), nxt(p, 2), nxt(p, 3)
            self.base = reserve(6)

        def go(self, half, index, owner, target):
            send(self.block(owner, half), self.land(index), self.base + index, target)

        def got(self, index, target):
            arrived(self.land(index), self.base + index, target)

        def add(self, owner, half, index):
            mine = self.block(owner, half)
            mine[...] = (mine[...].astype(F32) + self.land(index)[...].astype(F32)).astype(BF)

        def start(self):
            self.go(0, 0, self.across, self.plus)
            self.go(1, 1, self.across, self.minus)
            self.go(1, 2, self.after, self.plus)
            self.go(0, 3, self.before, self.minus)

        def mid(self):
            self.got(0, self.plus)
            self.add(self.after, 0, 0)
            self.go(0, 4, self.after, self.plus)
            self.got(1, self.minus)
            self.add(self.before, 1, 1)
            self.go(1, 5, self.before, self.minus)

        def end(self, store):
            for index in (2, 3, 4, 5):
                self.got(index, self.plus if index in (2, 4) else self.minus)
            for half, parts in ((0, (3, 4)), (1, (2, 5))):
                total = self.block(self.here, half)[...].astype(F32)
                for index in parts:
                    total = total + self.land(index)[...].astype(F32)
                store(half, total)

    def gathers(weight):
        cols_a, cols_b = COLS
        one_a = Gather("y", lambda p, h: weight.at[z, rows_at(p * 128 + h * 64, 64), cols_a])
        one_b = Gather("z", lambda p, h: weight.at[p, rows_at(y * 128 + h * 64, 64), cols_b])
        two_a = Gather("z", lambda p, h: weight.at[p, pl.ds(h * 256, 256), cols_a])
        two_b = Gather("y", lambda p, h: weight.at[pl.ds(h * 2, 2), rows_at(p * 128, 128), cols_b])
        return one_a, one_b, two_a, two_b

    class GradSum:
        def __init__(self, grad, which, accum, out):
            cols_a, cols_b = COLS
            self.grad, self.accum, self.out = grad, accum, out
            self.one_a = Scatter(
                "z", lambda p, h: grad.at[p, pl.ds(h * 256, 256), cols_a],
                lambda i: land_z.at[which, i],
            )
            self.one_b = Scatter(
                "y", lambda p, h: grad.at[pl.ds(h * 2, 2), rows_at(p * 128, 128), cols_b],
                lambda i: land_y.at[which, i],
            )
            self.two_a = Scatter(
                "y", lambda p, h: grad.at[z, rows_at(p * 128 + h * 64, 64), cols_a],
                lambda i: land_2.at[which, 0, i],
            )
            self.two_b = Scatter(
                "z", lambda p, h: grad.at[p, rows_at(y * 128 + h * 64, 64), cols_b],
                lambda i: land_2.at[which, 1, i],
            )

        def start(self):
            self.one_a.start()
            self.one_b.start()

        def mid(self):
            self.one_a.mid()
            self.one_b.mid()

        def turn(self):
            for ring in (self.one_a, self.one_b):
                def keep(half, total, ring=ring):
                    ring.block(ring.here, half)[...] = total.astype(BF)
                ring.end(keep)
            self.two_a.start()
            self.two_b.start()

        def mid_2(self):
            self.two_a.mid()
            self.two_b.mid()

        def end(self):
            for ring, cols in ((self.two_a, COLS[0]), (self.two_b, COLS[1])):
                def keep(half, total, cols=cols):
                    rows = pl.ds(half * 64, 64)
                    self.out[rows, cols] = self.accum[rows, cols] + 0.0078125 * total
                ring.end(keep)

    class TokenSum:
        def __init__(self, part, which, out):
            self.part, self.which, self.out = part, which, out
            self.base = reserve(4)
            self.order = (nxt(x, 2), nxt(x, 1), nxt(x, 3), x)
            self.ring = Scatter(
                "x", lambda p, h: part.at[p, rows_at(core * 128 + h * 64, 64), :],
                lambda i: land_x.at[which, i],
            )

        def offer(self, step):
            chunk = self.order[step]
            send(
                self.part.at[chunk, rows_at((1 - core) * 128, 128), :],
                land_pair.at[self.which, step],
                self.base + step,
                to["pair"],
            )

        def join(self, step):
            chunk = self.order[step]
            landed = land_pair.at[self.which, step]
            arrived(landed, self.base + step, to["pair"])
            mine = self.part.at[chunk, rows_at(core * 128, 128), :]
            mine[...] = (mine[...].astype(F32) + landed[...].astype(F32)).astype(BF)

        def end(self):
            def keep(half, total):
                self.out[pl.ds(half * 64, 64), :] = total.astype(BF)
            self.ring.end(keep)

    loads = [
        pltpu.make_async_copy(up_hbm, up_w.at[z, rows_at(y * 128, 128), :], load_sem.at[0]),
        pltpu.make_async_copy(down_hbm, down_w.at[z, rows_at(y * 128, 128), :], load_sem.at[1]),
        pltpu.make_async_copy(saved_hbm, saved, load_sem.at[2]),
        pltpu.make_async_copy(upstream_hbm, upstream, load_sem.at[3]),
        pltpu.make_async_copy(fresh_hbm, fresh, load_sem.at[4]),
        pltpu.make_async_copy(accum_up_hbm, accum_up, load_sem.at[5]),
        pltpu.make_async_copy(accum_down_hbm, accum_down, load_sem.at[6]),
    ]
    for load in loads:
        load.start()

    barrier = pltpu.get_barrier_semaphore()
    for target in to.values():
        pl.semaphore_signal(barrier, inc=1, device_id=target, device_id_type=MESH)
    pl.semaphore_wait(barrier, len(to))

    up_1a, up_1b, up_2a, up_2b = gathers(up_w)
    down_1a, down_1b, down_2a, down_2b = gathers(down_w)
    down_sum = GradSum(grad_down, 0, accum_down, accum_down_out)
    up_sum = GradSum(grad_up, 1, accum_up, accum_up_out)
    fresh_sum = TokenSum(fresh, 0, fresh_out)
    saved_sum = TokenSum(saved, 1, saved_grad)

    def forward(rows, store):
        def step(j, carry):
            i, n = j // 2, j % 2
            tile = rows[pl.ds(i * 2, 2)].reshape(512, 2048)
            cols = rows_at(n * 512, 512)
            pre = jnp.dot(
                tile, up_w[:, :, cols].reshape(2048, 512), preferred_element_type=F32
            )
            store(rows_at(i * 512, 512), cols, jnp.maximum(pre, 0.0))
            return carry
        lax.fori_loop(0, 4, step, 0)

    def keep_saved(at, cols, active):
        saved_active[at, cols] = active.astype(BF)
        saved_hidden[at, cols] = (active * active).astype(BF)

    def keep_fresh(at, cols, active):
        fresh_hidden[at, cols] = (active * active).astype(BF)

    def weight_grad(left, right, grad):
        def step(j, carry):
            cols = rows_at(j * 512, 512)
            tile = left(cols)
            total = lax.dot_general(
                tile, right[...], (((0,), (0,)), ((), ())), preferred_element_type=F32
            )
            grad[j] = total.astype(BF)
            return carry
        lax.fori_loop(0, 4, step, 0)

    def output_chunk(hidden, weight, part, chunk):
        def step(n, carry):
            total = lax.dot_general(
                hidden[rows_at(chunk * 256, 256), :], weight[n],
                (((1,), (1,)), ((), ())), preferred_element_type=F32,
            )
            part[chunk, :, rows_at(n * 512, 512)] = total.astype(BF)
            return carry
        lax.fori_loop(0, 4, step, 0)

    loads[0].wait()
    loads[1].wait()
    up_1a.start()
    up_1b.start()
    down_1a.start()
    down_1b.start()
    up_1a.mid()
    up_1b.mid()
    up_1a.end()
    up_1b.end()
    up_2a.start()
    up_2b.start()
    down_1a.mid()
    down_1b.mid()
    down_1a.end()
    down_1b.end()
    up_2a.mid()
    up_2b.mid()
    down_2a.start()
    down_2b.start()
    for load in loads[2:]:
        load.wait()
    up_2a.end()
    up_2b.end()

    forward(saved, keep_saved)
    down_2a.mid()
    down_2b.mid()
    weight_grad(lambda cols: upstream[:, cols], saved_hidden, grad_down)
    down_sum.start()
    forward(fresh, keep_fresh)
    down_2a.end()
    down_2b.end()

    for step in range(4):
        output_chunk(fresh_hidden, down_w, fresh, fresh_sum.order[step])
        fresh_sum.offer(step)
        if step == 1:
            down_sum.mid()
    for step in range(4):
        fresh_sum.join(step)
    fresh_sum.ring.start()

    def backward(j, carry):
        i, n = j // 2, j % 2
        at, cols = rows_at(i * 512, 512), rows_at(n * 512, 512)
        hidden_grad = jnp.dot(
            upstream[at, :], down_w[:, :, cols].reshape(2048, 512), preferred_element_type=F32
        )
        pre_grad[at, cols] = (2.0 * saved_active[at, cols].astype(F32) * hidden_grad).astype(BF)
        return carry
    lax.fori_loop(0, 4, backward, 0)
    fresh_sum.ring.mid()
    down_sum.turn()
    weight_grad(lambda cols: saved[:, :, cols].reshape(1024, 512), pre_grad, grad_up)
    up_sum.start()
    down_sum.mid_2()

    for step in range(4):
        output_chunk(pre_grad, up_w, saved, saved_sum.order[step])
        saved_sum.offer(step)
    fresh_sum.end()
    for step in range(4):
        saved_sum.join(step)
    saved_sum.ring.start()
    up_sum.mid()
    down_sum.end()
    saved_sum.ring.mid()
    up_sum.turn()
    up_sum.mid_2()
    saved_sum.end()
    up_sum.end()
    for copy in sent:
        copy.wait_send()


def body(fresh_rows, saved_rows, upstream_grad, proj_up, proj_down, accum_up, accum_down):
    anywhere = pl.BlockSpec(memory_space=pl.ANY)
    inside = pl.BlockSpec(memory_space=pltpu.VMEM)
    shape = jax.ShapeDtypeStruct
    return pl.pallas_call(
        kernel,
        out_shape=(
            shape((128, 2048), BF), shape((128, 2048), BF),
            shape((128, 1024), F32), shape((128, 1024), F32),
        ),
        in_specs=[anywhere] * 7,
        out_specs=(inside,) * 4,
        scratch_shapes=[
            pltpu.VMEM((4, 256, 2048), BF),
            pltpu.VMEM((4, 256, 2048), BF),
            pltpu.VMEM((1024, 2048), BF),
            pltpu.VMEM((4, 512, 1024), BF),
            pltpu.VMEM((4, 512, 1024), BF),
            pltpu.VMEM((128, 1024), F32),
            pltpu.VMEM((128, 1024), F32),
            pltpu.VMEM((1024, 1024), BF),
            pltpu.VMEM((1024, 1024), BF),
            pltpu.VMEM((1024, 1024), BF),
            pltpu.VMEM((1024, 1024), BF),
            pltpu.VMEM((4, 512, 1024), BF),
            pltpu.VMEM((4, 512, 1024), BF),
            pltpu.VMEM((2, 6, 256, 512), BF),
            pltpu.VMEM((2, 6, 2, 128, 512), BF),
            pltpu.VMEM((2, 2, 6, 64, 512), BF),
            pltpu.VMEM((2, 4, 128, 2048), BF),
            pltpu.VMEM((2, 6, 64, 2048), BF),
            pltpu.SemaphoreType.DMA((N_MSG,)),
            pltpu.SemaphoreType.DMA((N_MSG,)),
            pltpu.SemaphoreType.DMA((7,)),
        ],
        compiler_params=pltpu.CompilerParams(
            collective_id=0, has_side_effects=True, vmem_limit_bytes=67043328
        ),
        cost_estimate=pl.CostEstimate(
            flops=30064771072, bytes_accessed=32 * 1024 * 1024, transcendentals=0
        ),
    )(
        fresh_rows.reshape(4, 256, 2048), saved_rows.reshape(4, 256, 2048), upstream_grad,
        proj_up, proj_down, accum_up, accum_down,
    )


def solution(mesh):
    in_specs = (
        P("fs", None),
        P("fs", None),
        P("fs", None),
        P("fs", "tp"),
        P("fs", "tp"),
        P("fs", "tp"),
        P("fs", "tp"),
    )
    out_specs = (P(("fs", "tp"), None), P(("fs", "tp"), None), P("fs", "tp"), P("fs", "tp"))
    return jax.shard_map(body, mesh=mesh, in_specs=in_specs, out_specs=out_specs, check_vma=False)
```

time: 277 us -> 121 us (0.44)
  waiting for transfers between devices: 169 us -> 0 us
  Pallas kernels: 0 us -> 113 us
  matrix products: 52.5 us -> 0 us
  other arithmetic: 14.8 us -> 0 us
  between operations: 13.9 us -> 0.64 us
  local copies, waits for them, and re-layouts: 20.5 us -> 7.53 us
  starting transfers between devices: 6.06 us -> 0 us
    pallas_call x0 -> x1, Pallas kernels: none -> 113 us  [body(): pl.pallas_call(kernel, out_shape=(shape((128, 2048), BF), shape((128, 204...]
    all_to_all x1 -> x0, waiting for transfers between devices: 93.3 us -> none  [sum_at_owner(): blocks = lax.all_to_all(split_up(array, dim, count), axis, 0, 0, tiled=True)]
    all_gather x1 -> x0, waiting for transfers between devices: 75.5 us -> none  [side_by_side(): lax.all_gather(both, axis, axis=dim, tiled=True)]
    dot_general x6 -> x0, matrix products: 52.5 us -> none  [the longest x2 23 us: against_rows(): lax.dot_general(left, right, (((1,), (1,)), ((), ())), preferred_element_...]
    unnamed x18 -> x4, local copies, waits for them, and re-layouts: 19.4 us -> 7.53 us
    another operation x1 -> x0, other arithmetic: 7.56 us -> none  [body(): jnp.stack((fresh_term, input_part), axis=1).astype(jnp.bfloat16)]
    all_to_all x1 -> x0, starting transfers between devices: 5.94 us -> none  [sum_at_owner(): blocks = lax.all_to_all(split_up(array, dim, count), axis, 0, 0, tiled=True)]
    reduce_sum x1 -> x0, other arithmetic: 5.28 us -> none  [sum_at_owner(): return jnp.sum(blocks.astype(jnp.float32), axis=0)]
  transfers between devices with their start and end apart: 4 -> 0, of which waited for: 2 -> 0; matrix products, arithmetic and copies ran while one was open for 22% -> 0% of each run, Pallas kernels for 0% -> 0%
where the time goes in v1:
time: 121 us
  Pallas kernels  113 us (93%)
  local copies, waits for them, and re-layouts  7.53 us (6%)
    pallas_call x1, Pallas kernels, body(): pl.pallas_call(kernel, out_shape=(shape((128, 2048), BF), shape((128, 204...  113 us
    unnamed x4, local copies, waits for them, and re-layouts  7.53 us

profile of v1, /device:TPU:1, one launch (start us, length us, event | category | flops | bytes accessed | tf_op | source)
XLA Modules:
  0.0 121.1 jit_solution(10515126983721180112)
XLA Ops:
  0.6 112.9 %shard_map.102 = (bf16[128,2048]{1,0:T(8,128)(2,1)}, bf16[128,2048]{1,0:T(8,128)(2,1)}, f32[128,1024]{1,0:T(8,128)}, f32[128,1024]{1,0:T(8,128)}) custom-call(bf16[4,256,2048]{2,1,0:T(8,128)(2,1)} %bitcast.2, bf16[4,256,2048]{2,1,0:T(8,128)(2,1)} %bitcast.3, bf16[1024,2048]{1,0:T(8,128)(2,1)} %upstream_hbm.1, bf16[128,1024]{1,0:T(8,128)(2,1)} %up_hbm.1, ...), custom_call_target="tpu_custom_call" | custom-call | flops 30064771072 | bytes 33554432 | tf_op jit(solution)/shard_map/pallas_call | solution.py:376
  113.6 1.9 %copy.15 = bf16[128,2048]{1,0:T(8,128)(2,1)} copy(bf16[128,2048]{1,0:T(8,128)(2,1)} %get-tuple-element.8) | data formatting | bytes 1048576
  115.5 1.9 %copy.16 = bf16[128,2048]{1,0:T(8,128)(2,1)} copy(bf16[128,2048]{1,0:T(8,128)(2,1)} %get-tuple-element.9) | data formatting | bytes 1048576
  117.3 1.9 %copy.17 = f32[128,1024]{1,0:T(8,128)} copy(f32[128,1024]{1,0:T(8,128)} %get-tuple-element.10) | data formatting | bytes 1048576
  119.2 1.9 %copy.18 = f32[128,1024]{1,0:T(8,128)} copy(f32[128,1024]{1,0:T(8,128)} %get-tuple-element.11) | data formatting | bytes 1048576

commit v2 on v1

--- a/solution.py
+++ b/solution.py
@@ -23,7 +23,7 @@
     fresh_hbm, saved_hbm, upstream_hbm, up_hbm, down_hbm, accum_up_hbm, accum_down_hbm,
     fresh_out, saved_grad, accum_up_out, accum_down_out,
     fresh, saved, upstream, up_w, down_w, accum_up, accum_down,
-    fresh_hidden, saved_active, saved_hidden, pre_grad, grad_down, grad_up,
+    saved_t, upstream_t, fresh_hidden, saved_active, saved_hidden, pre_grad, grad_down,
     land_z, land_y, land_2, land_pair, land_x,
     send_sem, recv_sem, load_sem,
 ):
@@ -86,6 +86,8 @@
         def start(self):
             self.go(0, 0, self.here, self.plus)
             self.go(1, 2, self.here, self.minus)
+
+        def rest(self):
             self.go(1, 1, self.here, self.plus)
             self.go(0, 3, self.here, self.minus)
 
@@ -122,6 +124,8 @@
         def start(self):
             self.go(0, 0, self.across, self.plus)
             self.go(1, 1, self.across, self.minus)
+
+        def rest(self):
             self.go(1, 2, self.after, self.plus)
             self.go(0, 3, self.before, self.minus)
 
@@ -175,6 +179,10 @@
             self.one_a.start()
             self.one_b.start()
 
+        def rest(self):
+            self.one_a.rest()
+            self.one_b.rest()
+
         def mid(self):
             self.one_a.mid()
             self.one_b.mid()
@@ -186,6 +194,8 @@
                 ring.end(keep)
             self.two_a.start()
             self.two_b.start()
+            self.two_a.rest()
+            self.two_b.rest()
 
         def mid_2(self):
             self.two_a.mid()
@@ -248,10 +258,17 @@
 
     up_1a, up_1b, up_2a, up_2b = gathers(up_w)
     down_1a, down_1b, down_2a, down_2b = gathers(down_w)
+    grad_up = upstream_t
     down_sum = GradSum(grad_down, 0, accum_down, accum_down_out)
     up_sum = GradSum(grad_up, 1, accum_up, accum_up_out)
     fresh_sum = TokenSum(fresh, 0, fresh_out)
     saved_sum = TokenSum(saved, 1, saved_grad)
+
+    def turned(rows, out):
+        def step(i, carry):
+            out[:, :, rows_at(i * 256, 256)] = rows[i].T.reshape(4, 512, 256)
+            return carry
+        lax.fori_loop(0, 4, step, 0)
 
     def forward(rows, store):
         def step(j, carry):
@@ -272,96 +289,122 @@
     def keep_fresh(at, cols, active):
         fresh_hidden[at, cols] = (active * active).astype(BF)
 
-    def weight_grad(left, right, grad):
+    def backward():
         def step(j, carry):
-            cols = rows_at(j * 512, 512)
-            tile = left(cols)
-            total = lax.dot_general(
-                tile, right[...], (((0,), (0,)), ((), ())), preferred_element_type=F32
-            )
-            grad[j] = total.astype(BF)
+            i, n = j // 2, j % 2
+            at, cols = rows_at(i * 512, 512), rows_at(n * 512, 512)
+            hidden_grad = jnp.dot(
+                upstream[pl.ds(i * 2, 2)].reshape(512, 2048),
+                down_w[:, :, cols].reshape(2048, 512), preferred_element_type=F32,
+            )
+            pre_grad[at, cols] = (2.0 * saved_active[at, cols].astype(F32) * hidden_grad).astype(BF)
             return carry
         lax.fori_loop(0, 4, step, 0)
 
-    def output_chunk(hidden, weight, part, chunk):
+    def grad_piece(left, right, out, by):
+        plane, block = nxt(z, by), rows_at(nxt(y, by) * 128, 128)
+        total = jnp.dot(left[plane], right[:, COLS[0]], preferred_element_type=F32)
+        out[plane, :, COLS[0]] = total.astype(BF)
+        total = jnp.dot(
+            left[:, block, :].reshape(512, 1024), right[:, COLS[1]], preferred_element_type=F32
+        )
+        out[:, block, COLS[1]] = total.astype(BF).reshape(4, 128, 512)
+
+    def output_pair(hidden, weight, part, chunks):
+        left = jnp.concatenate([hidden[rows_at(c * 256, 256), :] for c in chunks], axis=0)
         def step(n, carry):
             total = lax.dot_general(
-                hidden[rows_at(chunk * 256, 256), :], weight[n],
-                (((1,), (1,)), ((), ())), preferred_element_type=F32,
-            )
-            part[chunk, :, rows_at(n * 512, 512)] = total.astype(BF)
+                left, weight[n], (((1,), (1,)), ((), ())), preferred_element_type=F32
+            ).astype(BF)
+            part[chunks[0], :, rows_at(n * 512, 512)] = total[:256]
+            part[chunks[1], :, rows_at(n * 512, 512)] = total[256:]
             return carry
         lax.fori_loop(0, 4, step, 0)
 
     loads[0].wait()
     loads[1].wait()
-    up_1a.start()
-    up_1b.start()
-    down_1a.start()
-    down_1b.start()
-    up_1a.mid()
-    up_1b.mid()
-    up_1a.end()
-    up_1b.end()
-    up_2a.start()
-    up_2b.start()
-    down_1a.mid()
-    down_1b.mid()
-    down_1a.end()
-    down_1b.end()
-    up_2a.mid()
-    up_2b.mid()
-    down_2a.start()
-    down_2b.start()
+    for ring in (up_1a, up_1b):
+        ring.start()
+    for ring in (up_1a, up_1b):
+        ring.rest()
+    for ring in (up_1a, up_1b):
+        ring.mid()
+    for ring in (down_1a, down_1b):
+        ring.start()
+        ring.rest()
     for load in loads[2:]:
         load.wait()
-    up_2a.end()
-    up_2b.end()
+    for ring in (up_1a, up_1b):
+        ring.end()
+    for ring in (up_2a, up_2b):
+        ring.start()
+    for ring in (down_1a, down_1b):
+        ring.mid()
+    for ring in (up_2a, up_2b):
+        ring.rest()
+    turned(upstream, upstream_t)
+    for ring in (up_2a, up_2b):
+        ring.mid()
+    for ring in (down_1a, down_1b):
+        ring.end()
+    for ring in (down_2a, down_2b):
+        ring.start()
+        ring.rest()
+    turned(saved, saved_t)
+    for ring in (up_2a, up_2b):
+        ring.end()
 
     forward(saved, keep_saved)
-    down_2a.mid()
-    down_2b.mid()
-    weight_grad(lambda cols: upstream[:, cols], saved_hidden, grad_down)
+    for ring in (down_2a, down_2b):
+        ring.mid()
+    for by in (2, 1, 3, 0):
+        grad_piece(upstream_t, saved_hidden, grad_down, by)
     down_sum.start()
+    down_sum.rest()
     forward(fresh, keep_fresh)
-    down_2a.end()
-    down_2b.end()
-
-    for step in range(4):
-        output_chunk(fresh_hidden, down_w, fresh, fresh_sum.order[step])
-        fresh_sum.offer(step)
-        if step == 1:
-            down_sum.mid()
-    for step in range(4):
-        fresh_sum.join(step)
+    for ring in (down_2a, down_2b):
+        ring.end()
+
+    output_pair(fresh_hidden, down_w, fresh, fresh_sum.order[:2])
+    fresh_sum.offer(0)
+    fresh_sum.offer(1)
+    output_pair(fresh_hidden, down_w, fresh, fresh_sum.order[2:])
+    fresh_sum.offer(2)
+    fresh_sum.offer(3)
+    fresh_sum.join(0)
     fresh_sum.ring.start()
-
-    def backward(j, carry):
-        i, n = j // 2, j % 2
-        at, cols = rows_at(i * 512, 512), rows_at(n * 512, 512)
-        hidden_grad = jnp.dot(
-            upstream[at, :], down_w[:, :, cols].reshape(2048, 512), preferred_element_type=F32
-        )
-        pre_grad[at, cols] = (2.0 * saved_active[at, cols].astype(F32) * hidden_grad).astype(BF)
-        return carry
-    lax.fori_loop(0, 4, backward, 0)
+    fresh_sum.join(1)
+    down_sum.mid()
+    fresh_sum.join(2)
+    fresh_sum.ring.rest()
+    backward()
+    fresh_sum.join(3)
     fresh_sum.ring.mid()
+    grad_piece(saved_t, pre_grad, grad_up, 2)
+    up_sum.start()
+    grad_piece(saved_t, pre_grad, grad_up, 1)
     down_sum.turn()
-    weight_grad(lambda cols: saved[:, :, cols].reshape(1024, 512), pre_grad, grad_up)
-    up_sum.start()
+    grad_piece(saved_t, pre_grad, grad_up, 3)
+    up_sum.rest()
+    grad_piece(saved_t, pre_grad, grad_up, 0)
+    output_pair(pre_grad, up_w, saved, saved_sum.order[:2])
+    saved_sum.offer(0)
+    saved_sum.offer(1)
+    up_sum.mid()
+    output_pair(pre_grad, up_w, saved, saved_sum.order[2:])
+    saved_sum.offer(2)
+    saved_sum.offer(3)
+    saved_sum.join(0)
+    saved_sum.ring.start()
+    saved_sum.join(1)
+    saved_sum.join(2)
+    saved_sum.ring.rest()
+    saved_sum.join(3)
     down_sum.mid_2()
-
-    for step in range(4):
-        output_chunk(pre_grad, up_w, saved, saved_sum.order[step])
-        saved_sum.offer(step)
     fresh_sum.end()
-    for step in range(4):
-        saved_sum.join(step)
-    saved_sum.ring.start()
-    up_sum.mid()
-    down_sum.end()
     saved_sum.ring.mid()
     up_sum.turn()
+    down_sum.end()
     up_sum.mid_2()
     saved_sum.end()
     up_sum.end()
@@ -369,11 +412,18 @@
         copy.wait_send()
 
 
+def settle(a, b, c, d, out_a, out_b, out_c, out_d):
+    out_a[...] = a[...]
+    out_b[...] = b[...]
+    out_c[...] = c[...]
+    out_d[...] = d[...]
+
+
 def body(fresh_rows, saved_rows, upstream_grad, proj_up, proj_down, accum_up, accum_down):
     anywhere = pl.BlockSpec(memory_space=pl.ANY)
     inside = pl.BlockSpec(memory_space=pltpu.VMEM)
     shape = jax.ShapeDtypeStruct
-    return pl.pallas_call(
+    results = pl.pallas_call(
         kernel,
         out_shape=(
             shape((128, 2048), BF), shape((128, 2048), BF),
@@ -384,16 +434,17 @@
         scratch_shapes=[
             pltpu.VMEM((4, 256, 2048), BF),
             pltpu.VMEM((4, 256, 2048), BF),
-            pltpu.VMEM((1024, 2048), BF),
+            pltpu.VMEM((4, 256, 2048), BF),
             pltpu.VMEM((4, 512, 1024), BF),
             pltpu.VMEM((4, 512, 1024), BF),
             pltpu.VMEM((128, 1024), F32),
             pltpu.VMEM((128, 1024), F32),
+            pltpu.VMEM((4, 512, 1024), BF),
+            pltpu.VMEM((4, 512, 1024), BF),
             pltpu.VMEM((1024, 1024), BF),
             pltpu.VMEM((1024, 1024), BF),
             pltpu.VMEM((1024, 1024), BF),
             pltpu.VMEM((1024, 1024), BF),
-            pltpu.VMEM((4, 512, 1024), BF),
             pltpu.VMEM((4, 512, 1024), BF),
             pltpu.VMEM((2, 6, 256, 512), BF),
             pltpu.VMEM((2, 6, 2, 128, 512), BF),
@@ -411,9 +462,16 @@
             flops=30064771072, bytes_accessed=32 * 1024 * 1024, transcendentals=0
         ),
     )(
-        fresh_rows.reshape(4, 256, 2048), saved_rows.reshape(4, 256, 2048), upstream_grad,
+        fresh_rows.reshape(4, 256, 2048), saved_rows.reshape(4, 256, 2048),
+        upstream_grad.reshape(4, 256, 2048),
         proj_up, proj_down, accum_up, accum_down,
     )
+    return pl.pallas_call(
+        settle,
+        out_shape=tuple(shape(r.shape, r.dtype) for r in results),
+        in_specs=[inside] * 4,
+        out_specs=(inside,) * 4,
+    )(*results)
 
 
 def solution(mesh):

time: 121 us -> 107 us (0.88); the launches traced: 121 us -> 106 us
  Pallas kernels: 113 us -> 105 us
  local copies, waits for them, and re-layouts: 7.53 us -> 0 us
    pallas_call x1, Pallas kernels: 113 us -> 102 us  [body(): pl.pallas_call(kernel, out_shape=(shape((128, 2048), BF), shape((128, 204...]
    unnamed x4 -> x0, local copies, waits for them, and re-layouts: 7.53 us -> none
    pallas_call x0 -> x1, Pallas kernels: none -> 2.86 us  [body(): pl.pallas_call(settle, out_shape=tuple((shape(r.shape, r.dtype) for r in...]
where the time goes in v2:
time: 107 us; the launch traced here: 106 us
  Pallas kernels  105 us (98%)
    pallas_call x1, Pallas kernels, body(): pl.pallas_call(kernel, out_shape=(shape((128, 2048), BF), shape((128, 204...  102 us
    pallas_call x1, Pallas kernels, body(): pl.pallas_call(settle, out_shape=tuple((shape(r.shape, r.dtype) for r in...  2.86 us

profile of v2, /device:TPU:1, one launch (start us, length us, event | category | flops | bytes accessed | tf_op | source)
XLA Modules:
  0.0 105.7 jit_solution(2839017956881976393)
XLA Ops:
  0.6 102.2 %shard_map.102 = (bf16[128,2048]{1,0:T(8,128)(2,1)}, bf16[128,2048]{1,0:T(8,128)(2,1)}, f32[128,1024]{1,0:T(8,128)}, f32[128,1024]{1,0:T(8,128)}) custom-call(bf16[4,256,2048]{2,1,0:T(8,128)(2,1)} %bitcast.3, bf16[4,256,2048]{2,1,0:T(8,128)(2,1)} %bitcast.4, bf16[4,256,2048]{2,1,0:T(8,128)(2,1)} %bitcast.5, bf16[128,1024]{1,0:T(8,128)(2,1)} %up_hbm.1, ...), custom_call_target="tpu_custom_call" | custom-call | flops 30064771072 | bytes 33554432 | tf_op jit(solution)/shard_map/pallas_call | solution.py:426
  102.8 2.9 %shard_map.103 = (bf16[128,2048]{1,0:T(8,128)(2,1)}, bf16[128,2048]{1,0:T(8,128)(2,1)}, f32[128,1024]{1,0:T(8,128)}, f32[128,1024]{1,0:T(8,128)}) custom-call(bf16[128,2048]{1,0:T(8,128)(2,1)} %get-tuple-element.8.a, bf16[128,2048]{1,0:T(8,128)(2,1)} %get-tuple-element.9.b, f32[128,1024]{1,0:T(8,128)} %get-tuple-element.10.c, f32[128,1024]{1,0:T(8,128)} %get-tuple-element.11.d), custom_call_target="tpu_custom_call" | custom-call | tf_op jit(solution)/shard_map/pallas_call | solution.py:469

commit v3 on v2

v3 whole, which is shorter than its diff:
```python
import jax
import jax.numpy as jnp
from jax import lax
from jax.experimental import pallas as pl
from jax.experimental.pallas import tpu as pltpu
from jax.sharding import PartitionSpec as P

MESH = pl.DeviceIdType.MESH
BF = jnp.bfloat16
F32 = jnp.float32
COLS = (slice(0, 512), slice(512, 1024))
GROUPS = tuple((slice(q, q + 256), slice(q + 512, q + 768)) for q in (0, 256))
N_RINGS = 12 + 16 + 2


def rows_at(start, size):
    return pl.ds(pl.multiple_of(start, size), size)


def kernel(
    fresh_hbm, saved_hbm, upstream_hbm, up_hbm, down_hbm, accum_up_hbm, accum_down_hbm,
    fresh_out, saved_grad, accum_up_out, accum_down_out,
    fresh, saved, upstream, up_w, down_w, accum_up, accum_down,
    saved_t, upstream_t, fresh_hidden, saved_active, saved_hidden, pre_grad, grad_down,
    land_z, land_y, land_2, land_pair, land_x,
    send_sem, recv_sem, load_sem,
):
    fs, tp = lax.axis_index("fs"), lax.axis_index("tp")
    z, y, x, core = fs // 4, fs % 4, tp // 2, tp % 2

    def nxt(p, by):
        return lax.rem(p + by, 4)

    to = {
        ("y", 1): (z * 4 + nxt(y, 1), tp),
        ("y", -1): (z * 4 + nxt(y, 3), tp),
        ("z", 1): (nxt(z, 1) * 4 + y, tp),
        ("z", -1): (nxt(z, 3) * 4 + y, tp),
        ("x", 1): (fs, nxt(x, 1) * 2 + core),
        ("x", -1): (fs, nxt(x, 3) * 2 + core),
        "pair": (fs, x * 2 + 1 - core),
    }
    place = {"y": y, "z": z, "x": x}
    used = [0]
    part_of = (slice(None), pl.ds(0, 480))
    bulks = (up_w.at[part_of], down_w.at[part_of], land_z, land_y, land_2, land_x, land_pair)

    def reserve(count):
        used[0] += count
        return used[0] - count

    def message(src, dst, sends, receives, target):
        return pltpu.make_async_remote_copy(
            src_ref=src,
            dst_ref=dst,
            send_sem=send_sem.at[sends],
            recv_sem=recv_sem.at[receives],
            device_id=target,
            device_id_type=MESH,
        )

    class Ring:
        def __init__(self, axis, pool):
            self.plus, self.minus = to[(axis, 1)], to[(axis, -1)]
            p = place[axis]
            self.here, self.after, self.across, self.before = p, nxt(p, 1), nxt(p, 2), nxt(p, 3)
            self.out, self.into = pool, reserve(3)

        def push(self, src, dst, slot, target):
            message(src, dst, self.out, self.into + slot, target).start()

        def got(self, dst, slot):
            message(dst, dst, self.out, self.into + slot, self.plus).wait_recv()

    class Gather(Ring):
        def __init__(self, axis, block, two, pool):
            super().__init__(axis, pool)
            self.block, self.two = block, two

        def go(self, half, slot, owner, target):
            part = self.block(owner, half)
            self.push(part, part, slot, target)

        def start(self):
            self.go(0, 0, self.here, self.plus)
            self.go(1, 1, self.here, self.minus)

        def rest(self):
            self.go(1, 2, self.here, self.plus)
            self.go(0, 2, self.here, self.minus)

        def mid(self):
            self.got(self.block(self.before, 0), 0)
            self.go(0, 2, self.before, self.plus)
            self.got(self.block(self.after, 1), 1)
            self.go(1, 2, self.after, self.minus)

        def end(self):
            self.got(self.two, 2)

    class Scatter(Ring):
        def __init__(self, axis, block, land, pool):
            super().__init__(axis, pool)
            self.block, self.land = block, land

        def go(self, half, slot, index, owner, target):
            self.push(self.block(owner, half), self.land.at[index], slot, target)

        def add(self, owner, half, index):
            mine = self.block(owner, half)
            mine[...] = (mine[...].astype(F32) + self.land[index].astype(F32)).astype(BF)

        def start(self):
            self.go(0, 0, 0, self.across, self.plus)
            self.go(1, 1, 1, self.across, self.minus)

        def rest(self):
            self.go(1, 2, 2, self.after, self.plus)
            self.go(0, 2, 3, self.before, self.minus)

        def mid(self):
            self.got(self.land.at[0], 0)
            self.add(self.after, 0, 0)
            self.go(0, 2, 4, self.after, self.plus)
            self.got(self.land.at[1], 1)
            self.add(self.before, 1, 1)
            self.go(1, 2, 5, self.before, self.minus)

        def end(self, store):
            self.got(self.land.at[pl.ds(2, 4)], 2)
            for half, parts in ((0, (3, 4)), (1, (2, 5))):
                total = self.block(self.here, half)[...].astype(F32)
                for index in parts:
                    total = total + self.land[index].astype(F32)
                store(half, total)

    class Both:
        def __init__(self, *rings):
            self.rings = rings

        def __getattr__(self, step):
            def run():
                for ring in self.rings:
                    getattr(ring, step)()
            return run

    def gather_1(w, pool):
        a, b = COLS
        return Both(
            Gather(
                "y", lambda p, h: w.at[z, rows_at(p * 128 + h * 64, 64), a],
                w.at[0, pl.ds(0, 256), a], pool,
            ),
            Gather(
                "z", lambda p, h: w.at[p, rows_at(y * 128 + h * 64, 64), b],
                w.at[0, pl.ds(0, 256), b], pool,
            ),
        )

    def gather_2(w, q, pool):
        a, b = GROUPS[q]
        return Both(
            Gather(
                "z", lambda p, h: w.at[p, pl.ds(h * 256, 256), a],
                w.at[pl.ds(0, 2), :, a], pool,
            ),
            Gather(
                "y", lambda p, h: w.at[pl.ds(h * 2, 2), rows_at(p * 128, 128), b],
                w.at[:, pl.ds(0, 256), b], pool,
            ),
        )

    class GradSum:
        def __init__(self, grad, which, q, accum, out):
            a, b = GROUPS[q]
            self.q, self.accum, self.out = q, accum, out
            self.one = (
                Scatter(
                    "z", lambda p, h: grad.at[p, pl.ds(h * 256, 256), a],
                    land_z.at[which, q], 2,
                ),
                Scatter(
                    "y", lambda p, h: grad.at[pl.ds(h * 2, 2), rows_at(p * 128, 128), b],
                    land_y.at[which, q], 3,
                ),
            )
            self.two = (
                Scatter(
                    "y", lambda p, h: grad.at[z, rows_at(p * 128 + h * 64, 64), a],
                    land_2.at[which, q, 0], 4,
                ),
                Scatter(
                    "z", lambda p, h: grad.at[p, rows_at(y * 128 + h * 64, 64), b],
                    land_2.at[which, q, 1], 4,
                ),
            )

        def start(self):
            for ring in self.one:
                ring.start()
            for ring in self.one:
                ring.rest()

        def mid(self):
            for ring in self.one:
                ring.mid()

        def turn(self):
            for ring, after in zip(self.one, self.two):
                def keep(half, total, ring=ring):
                    ring.block(ring.here, half)[...] = total.astype(BF)
                ring.end(keep)
                after.start()
                after.rest()

        def mid_2(self):
            for ring in self.two:
                ring.mid()

        def end(self):
            for ring, cols in zip(self.two, GROUPS[self.q]):
                def keep(half, total, cols=cols):
                    rows = pl.ds(half * 64, 64)
                    self.out[rows, cols] = self.accum[rows, cols] + 0.0078125 * total
                ring.end(keep)

    class TokenSum:
        def __init__(self, part, which, out):
            self.part, self.which, self.out = part, which, out
            self.receives = reserve(4)
            self.order = (nxt(x, 2), nxt(x, 1), nxt(x, 3), x)
            self.ring = Scatter(
                "x", lambda p, h: part.at[p, rows_at(core * 128 + h * 64, 64), :],
                land_x.at[which], 5,
            )

        def pair(self, src, step):
            return message(
                src, land_pair.at[self.which, step],
                6, self.receives + step, to["pair"],
            )

        def offer(self, *steps):
            for step in steps:
                theirs = self.part.at[self.order[step], rows_at((1 - core) * 128, 128), :]
                self.pair(theirs, step).start()

        def join(self, step):
            landed = land_pair.at[self.which, step]
            self.pair(landed, step).wait_recv()
            mine = self.part.at[self.order[step], rows_at(core * 128, 128), :]
            mine[...] = (mine[...].astype(F32) + landed[...].astype(F32)).astype(BF)

        def end(self):
            def keep(half, total):
                self.out[pl.ds(half * 64, 64), :] = total.astype(BF)
            self.ring.end(keep)

    loads = [
        pltpu.make_async_copy(up_hbm, up_w.at[z, rows_at(y * 128, 128), :], load_sem.at[0]),
        pltpu.make_async_copy(down_hbm, down_w.at[z, rows_at(y * 128, 128), :], load_sem.at[1]),
        pltpu.make_async_copy(saved_hbm, saved, load_sem.at[2]),
        pltpu.make_async_copy(upstream_hbm, upstream, load_sem.at[3]),
        pltpu.make_async_copy(fresh_hbm, fresh, load_sem.at[4]),
        pltpu.make_async_copy(accum_up_hbm, accum_up, load_sem.at[5]),
        pltpu.make_async_copy(accum_down_hbm, accum_down, load_sem.at[6]),
    ]
    for load in loads:
        load.start()

    barrier = pltpu.get_barrier_semaphore()
    for target in to.values():
        pl.semaphore_signal(barrier, inc=1, device_id=target, device_id_type=MESH)
    pl.semaphore_wait(barrier, len(to))

    up_1, up_2 = gather_1(up_w, 0), (gather_2(up_w, 0, 0), gather_2(up_w, 1, 0))
    down_1, down_2 = gather_1(down_w, 1), (gather_2(down_w, 0, 1), gather_2(down_w, 1, 1))
    grad_up = upstream_t
    down_sum = [GradSum(grad_down, 0, q, accum_down, accum_down_out) for q in range(2)]
    up_sum = [GradSum(grad_up, 1, q, accum_up, accum_up_out) for q in range(2)]
    fresh_sum = TokenSum(fresh, 0, fresh_out)
    saved_sum = TokenSum(saved, 1, saved_grad)

    def turned(rows, out):
        def step(i, carry):
            out[:, :, rows_at(i * 256, 256)] = rows[i].T.reshape(4, 512, 256)
            return carry
        lax.fori_loop(0, 4, step, 0)

    def hidden(q, rows, weight, store, first=0, last=4):
        def step(j, carry):
            i, ab = j // 2, j % 2
            cols = rows_at(ab * 512 + q * 256, 256)
            pre = jnp.dot(
                rows[pl.ds(i * 2, 2)].reshape(512, 2048),
                weight[:, :, cols].reshape(2048, 256), preferred_element_type=F32,
            )
            store(rows_at(i * 512, 512), cols, pre)
            return carry
        lax.fori_loop(first, last, step, 0)

    def keep_saved(at, cols, pre):
        active = jnp.maximum(pre, 0.0)
        saved_active[at, cols] = active.astype(BF)
        saved_hidden[at, cols] = (active * active).astype(BF)

    def keep_fresh(at, cols, pre):
        active = jnp.maximum(pre, 0.0)
        fresh_hidden[at, cols] = (active * active).astype(BF)

    def keep_back(at, cols, hidden_grad):
        active = saved_active[at, cols].astype(F32)
        pre_grad[at, cols] = (2.0 * active * hidden_grad).astype(BF)

    def grad(q, left, right, out, first=0, last=4):
        a, b = GROUPS[q]
        def step(p, carry):
            total = jnp.dot(left[p], right[:, a], preferred_element_type=F32)
            out[p, :, a] = total.astype(BF)
            total = jnp.dot(left[p], right[:, b], preferred_element_type=F32)
            out[p, :, b] = total.astype(BF)
            return carry
        lax.fori_loop(first, last, step, 0)

    def output(q, hidden_rows, weight, part, chunks, first=0, last=4):
        def beside(block):
            if q is None:
                return block[...]
            a, b = GROUPS[q]
            return jnp.concatenate([block[:, a], block[:, b]], axis=1)
        def step(n, carry):
            left = jnp.concatenate(
                [beside(hidden_rows.at[rows_at(c * 256, 256)]) for c in chunks], axis=0
            )
            total = lax.dot_general(
                left, beside(weight.at[n]), (((1,), (1,)), ((), ())), preferred_element_type=F32
            )
            cols = rows_at(n * 512, 512)
            for k, c in enumerate(chunks):
                some = total[k * 256:k * 256 + 256]
                if q == 1:
                    some = part[c, :, cols].astype(F32) + some
                part[c, :, cols] = some.astype(BF)
            return carry
        lax.fori_loop(first, last, step, 0)

    loads[0].wait()
    loads[1].wait()
    up_1.start()
    up_1.rest()
    up_1.mid()
    down_1.start()
    down_1.rest()
    for load in loads[2:]:
        load.wait()
    up_1.end()
    up_2[0].start()
    down_1.mid()
    up_2[0].rest()
    turned(upstream, upstream_t)
    up_2[0].mid()
    up_2[1].start()
    up_2[1].rest()
    down_1.end()
    turned(saved, saved_t)
    up_2[0].end()

    hidden(0, saved, up_w, keep_saved)
    up_2[1].mid()
    down_2[0].start()
    down_2[0].rest()
    hidden(0, fresh, up_w, keep_fresh)
    grad(0, upstream_t, saved_hidden, grad_down)
    up_2[1].end()
    hidden(1, saved, up_w, keep_saved)
    down_2[0].mid()
    down_2[1].start()
    down_2[1].rest()
    grad(1, upstream_t, saved_hidden, grad_down)
    hidden(1, fresh, up_w, keep_fresh)
    down_2[0].end()
    output(0, fresh_hidden, down_w, fresh, fresh_sum.order[:2])
    down_2[1].mid()
    output(0, fresh_hidden, down_w, fresh, fresh_sum.order[2:])
    pl.when(core == 0)(down_sum[0].start)
    down_2[1].end()

    pl.when(core == 1)(down_sum[0].start)
    down_sum[1].start()
    output(1, fresh_hidden, down_w, fresh, fresh_sum.order[:2])
    fresh_sum.offer(0, 1)
    output(1, fresh_hidden, down_w, fresh, fresh_sum.order[2:])
    fresh_sum.offer(2, 3)
    fresh_sum.join(0)
    fresh_sum.ring.start()
    hidden(0, upstream, down_w, keep_back)
    fresh_sum.join(1)
    fresh_sum.join(2)
    fresh_sum.ring.rest()
    fresh_sum.join(3)
    down_sum[0].mid()
    grad(0, saved_t, pre_grad, grad_up)
    up_sum[0].start()
    hidden(1, upstream, down_w, keep_back, 0, 2)
    fresh_sum.ring.mid()
    down_sum[1].mid()
    hidden(1, upstream, down_w, keep_back, 2, 4)
    grad(1, saved_t, pre_grad, grad_up)
    up_sum[1].start()
    output(None, pre_grad, up_w, saved, saved_sum.order[:2])
    saved_sum.offer(0, 1)
    output(None, pre_grad, up_w, saved, saved_sum.order[2:], 0, 2)
    saved_sum.join(0)
    saved_sum.ring.start()
    saved_sum.join(1)
    up_sum[0].mid()
    output(None, pre_grad, up_w, saved, saved_sum.order[2:], 2, 4)
    saved_sum.offer(2, 3)
    down_sum[0].turn()
    saved_sum.join(2)
    saved_sum.ring.rest()
    saved_sum.join(3)
    fresh_sum.end()
    up_sum[1].mid()
    down_sum[1].turn()
    saved_sum.ring.mid()
    down_sum[0].mid_2()
    up_sum[0].turn()
    up_sum[1].turn()
    down_sum[1].mid_2()
    up_sum[0].mid_2()
    up_sum[1].mid_2()
    down_sum[0].end()
    down_sum[1].end()
    up_sum[0].end()
    saved_sum.end()
    up_sum[1].end()
    for index, bulk in enumerate(bulks):
        message(bulk, bulk, index, 0, to["pair"]).wait_send()


def settle(*refs):
    held, out, sems = refs[:4], refs[4:8], refs[8]
    copies = [pltpu.make_async_copy(h, o, sems.at[i]) for i, (h, o) in enumerate(zip(held, out))]
    for copy in copies:
        copy.start()
    for copy in copies:
        copy.wait()


def body(fresh_rows, saved_rows, upstream_grad, proj_up, proj_down, accum_up, accum_down):
    anywhere = pl.BlockSpec(memory_space=pl.ANY)
    inside = pl.BlockSpec(memory_space=pltpu.VMEM)
    shape = jax.ShapeDtypeStruct
    results = pl.pallas_call(
        kernel,
        out_shape=(
            pltpu.VMEM((128, 2048), BF), pltpu.VMEM((128, 2048), BF),
            pltpu.VMEM((128, 1024), F32), pltpu.VMEM((128, 1024), F32),
        ),
        in_specs=[anywhere] * 7,
        out_specs=(inside,) * 4,
        scratch_shapes=[
            pltpu.VMEM((4, 256, 2048), BF),
            pltpu.VMEM((4, 256, 2048), BF),
            pltpu.VMEM((4, 256, 2048), BF),
            pltpu.VMEM((4, 512, 1024), BF),
            pltpu.VMEM((4, 512, 1024), BF),
            pltpu.VMEM((128, 1024), F32),
            pltpu.VMEM((128, 1024), F32),
            pltpu.VMEM((4, 512, 1024), BF),
            pltpu.VMEM((4, 512, 1024), BF),
            pltpu.VMEM((1024, 1024), BF),
            pltpu.VMEM((1024, 1024), BF),
            pltpu.VMEM((1024, 1024), BF),
            pltpu.VMEM((1024, 1024), BF),
            pltpu.VMEM((4, 512, 1024), BF),
            pltpu.VMEM((2, 2, 6, 256, 256), BF),
            pltpu.VMEM((2, 2, 6, 2, 128, 256), BF),
            pltpu.VMEM((2, 2, 2, 6, 64, 256), BF),
            pltpu.VMEM((2, 4, 128, 2048), BF),
            pltpu.VMEM((2, 6, 64, 2048), BF),
            pltpu.SemaphoreType.DMA((7,)),
            pltpu.SemaphoreType.DMA((N_RINGS * 3 + 8,)),
            pltpu.SemaphoreType.DMA((7,)),
        ],
        compiler_params=pltpu.CompilerParams(
            collective_id=0, has_side_effects=True, vmem_limit_bytes=62914560
        ),
        cost_estimate=pl.CostEstimate(
            flops=30064771072, bytes_accessed=32 * 1024 * 1024, transcendentals=0
        ),
    )(
        fresh_rows.reshape(4, 256, 2048), saved_rows.reshape(4, 256, 2048),
        upstream_grad.reshape(4, 256, 2048),
        proj_up, proj_down, accum_up, accum_down,
    )
    return pl.pallas_call(
        settle,
        out_shape=tuple(shape(r.shape, r.dtype) for r in results),
        in_specs=[inside] * 4,
        out_specs=(anywhere,) * 4,
        scratch_shapes=[pltpu.SemaphoreType.DMA((4,))],
    )(*[pltpu.with_memory_space_constraint(r, pltpu.VMEM) for r in results])


def solution(mesh):
    in_specs = (
        P("fs", None),
        P("fs", None),
        P("fs", None),
        P("fs", "tp"),
        P("fs", "tp"),
        P("fs", "tp"),
        P("fs", "tp"),
    )
    out_specs = (P(("fs", "tp"), None), P(("fs", "tp"), None), P("fs", "tp"), P("fs", "tp"))
    return jax.shard_map(body, mesh=mesh, in_specs=in_specs, out_specs=out_specs, check_vma=False)
```

time: 107 us -> 99.8 us (0.933)
  Pallas kernels: 105 us -> 97.8 us
    pallas_call x1, Pallas kernels: 102 us -> 96.5 us  [body(): pl.pallas_call(kernel, out_shape=(pltpu.VMEM((128, 2048), BF), pltpu.VMEM...]
    pallas_call x1, Pallas kernels: 2.86 us -> 1.35 us  [body(): pl.pallas_call(settle, out_shape=tuple((shape(r.shape, r.dtype) for r in...]
where the time goes in v3:
time: 99.8 us; the launch traced here: 98.6 us
  Pallas kernels  97.8 us (98%)
    pallas_call x1, Pallas kernels, body(): pl.pallas_call(kernel, out_shape=(pltpu.VMEM((128, 2048), BF), pltpu.VMEM...  96.5 us

profile of v3, /device:TPU:1, one launch (start us, length us, event | category | flops | bytes accessed | tf_op | source)
XLA Modules:
  0.0 98.6 jit_solution(18004773224245326109)
XLA Ops:
  0.6 96.5 %shard_map.102 = (bf16[128,2048]{1,0:T(8,128)(2,1)S(1)}, bf16[128,2048]{1,0:T(8,128)(2,1)S(1)}, f32[128,1024]{1,0:T(8,128)S(1)}, f32[128,1024]{1,0:T(8,128)S(1)}) custom-call(bf16[4,256,2048]{2,1,0:T(8,128)(2,1)} %bitcast.3, bf16[4,256,2048]{2,1,0:T(8,128)(2,1)} %bitcast.4, bf16[4,256,2048]{2,1,0:T(8,128)(2,1)} %bitcast.5, bf16[128,1024]{1,0:T(8,128)(2,1)} %up_hbm.1, ...), custom_call_target="tpu_custom_call" | custom-call | flops 30064771072 | bytes 33554432 | tf_op jit(solution)/shard_map/pallas_call | solution.py:455
  97.1 1.3 %shard_map.103 = (bf16[128,2048]{1,0:T(8,128)(2,1)}, bf16[128,2048]{1,0:T(8,128)(2,1)}, f32[128,1024]{1,0:T(8,128)}, f32[128,1024]{1,0:T(8,128)}) custom-call(bf16[128,2048]{1,0:T(8,128)(2,1)S(1)} %get-tuple-element.8.refs_0_, bf16[128,2048]{1,0:T(8,128)(2,1)S(1)} %get-tuple-element.9.refs_1_, f32[128,1024]{1,0:T(8,128)S(1)} %get-tuple-element.10.refs_2_, ...), custom_call_target="tpu_custom_call" | custom-call | tf_op jit(solution)/shard_map/pallas_call | solution.py:498

commit v4 on v3

--- a/solution.py
+++ b/solution.py
@@ -10,7 +10,7 @@
 F32 = jnp.float32
 COLS = (slice(0, 512), slice(512, 1024))
 GROUPS = tuple((slice(q, q + 256), slice(q + 512, q + 768)) for q in (0, 256))
-N_RINGS = 12 + 16 + 2
+N_RINGS = 14 + 16 + 2
 
 
 def rows_at(start, size):
@@ -144,8 +144,8 @@
                     getattr(ring, step)()
             return run
 
-    def gather_1(w, pool):
-        a, b = COLS
+    def gather_1(w, cols, pool):
+        a, b = cols
         return Both(
             Gather(
                 "y", lambda p, h: w.at[z, rows_at(p * 128 + h * 64, 64), a],
@@ -273,8 +273,9 @@
         pl.semaphore_signal(barrier, inc=1, device_id=target, device_id_type=MESH)
     pl.semaphore_wait(barrier, len(to))
 
-    up_1, up_2 = gather_1(up_w, 0), (gather_2(up_w, 0, 0), gather_2(up_w, 1, 0))
-    down_1, down_2 = gather_1(down_w, 1), (gather_2(down_w, 0, 1), gather_2(down_w, 1, 1))
+    up_1 = [gather_1(up_w, cols, 0) for cols in GROUPS]
+    up_2, down_1 = (gather_2(up_w, 0, 0), gather_2(up_w, 1, 0)), gather_1(down_w, COLS, 1)
+    down_2 = (gather_2(down_w, 0, 1), gather_2(down_w, 1, 1))
     grad_up = upstream_t
     down_sum = [GradSum(grad_down, 0, q, accum_down, accum_down_out) for q in range(2)]
     up_sum = [GradSum(grad_up, 1, q, accum_up, accum_up_out) for q in range(2)]
@@ -346,19 +347,22 @@
 
     loads[0].wait()
     loads[1].wait()
-    up_1.start()
-    up_1.rest()
-    up_1.mid()
+    for ring in up_1:
+        ring.start()
+        ring.rest()
+    up_1[0].mid()
     down_1.start()
     down_1.rest()
+    up_1[1].mid()
     for load in loads[2:]:
         load.wait()
-    up_1.end()
+    up_1[0].end()
     up_2[0].start()
     down_1.mid()
     up_2[0].rest()
     turned(upstream, upstream_t)
     up_2[0].mid()
+    up_1[1].end()
     up_2[1].start()
     up_2[1].rest()
     down_1.end()
@@ -384,15 +388,18 @@
     output(0, fresh_hidden, down_w, fresh, fresh_sum.order[2:])
     pl.when(core == 0)(down_sum[0].start)
     down_2[1].end()
-
     pl.when(core == 1)(down_sum[0].start)
+
+    output(1, fresh_hidden, down_w, fresh, fresh_sum.order[:1])
+    fresh_sum.offer(0)
+    output(1, fresh_hidden, down_w, fresh, fresh_sum.order[1:2])
+    fresh_sum.offer(1)
     down_sum[1].start()
-    output(1, fresh_hidden, down_w, fresh, fresh_sum.order[:2])
-    fresh_sum.offer(0, 1)
-    output(1, fresh_hidden, down_w, fresh, fresh_sum.order[2:])
-    fresh_sum.offer(2, 3)
+    output(1, fresh_hidden, down_w, fresh, fresh_sum.order[2:], 0, 2)
     fresh_sum.join(0)
     fresh_sum.ring.start()
+    output(1, fresh_hidden, down_w, fresh, fresh_sum.order[2:], 2, 4)
+    fresh_sum.offer(2, 3)
     hidden(0, upstream, down_w, keep_back)
     fresh_sum.join(1)
     fresh_sum.join(2)

time: 99.8 us -> 99.5 us (level)
  no operation moved by 1% of the time
where the time goes in v4:
time: 99.5 us; the launch traced here: 98.7 us
  Pallas kernels  97.9 us (98%)
    pallas_call x1, Pallas kernels, body(): pl.pallas_call(kernel, out_shape=(pltpu.VMEM((128, 2048), BF), pltpu.VMEM...  96.6 us

profile of v4, /device:TPU:1, one launch (start us, length us, event | category | flops | bytes accessed | tf_op | source)
XLA Modules:
  0.0 98.7 jit_solution(9114602512781248774)
XLA Ops:
  0.6 96.6 %shard_map.102 = (bf16[128,2048]{1,0:T(8,128)(2,1)S(1)}, bf16[128,2048]{1,0:T(8,128)(2,1)S(1)}, f32[128,1024]{1,0:T(8,128)S(1)}, f32[128,1024]{1,0:T(8,128)S(1)}) custom-call(bf16[4,256,2048]{2,1,0:T(8,128)(2,1)} %bitcast.3, bf16[4,256,2048]{2,1,0:T(8,128)(2,1)} %bitcast.4, bf16[4,256,2048]{2,1,0:T(8,128)(2,1)} %bitcast.5, bf16[128,1024]{1,0:T(8,128)(2,1)} %up_hbm.1, ...), custom_call_target="tpu_custom_call" | custom-call | flops 30064771072 | bytes 33554432 | tf_op jit(solution)/shard_map/pallas_call | solution.py:462
  97.2 1.3 %shard_map.103 = (bf16[128,2048]{1,0:T(8,128)(2,1)}, bf16[128,2048]{1,0:T(8,128)(2,1)}, f32[128,1024]{1,0:T(8,128)}, f32[128,1024]{1,0:T(8,128)}) custom-call(bf16[128,2048]{1,0:T(8,128)(2,1)S(1)} %get-tuple-element.8.refs_0_, bf16[128,2048]{1,0:T(8,128)(2,1)S(1)} %get-tuple-element.9.refs_1_, f32[128,1024]{1,0:T(8,128)S(1)} %get-tuple-element.10.refs_2_, ...), custom_call_target="tpu_custom_call" | custom-call | tf_op jit(solution)/shard_map/pallas_call | solution.py:505

commit v5 on v4

--- a/solution.py
+++ b/solution.py
@@ -388,13 +388,13 @@
     output(0, fresh_hidden, down_w, fresh, fresh_sum.order[2:])
     pl.when(core == 0)(down_sum[0].start)
     down_2[1].end()
-    pl.when(core == 1)(down_sum[0].start)
 
     output(1, fresh_hidden, down_w, fresh, fresh_sum.order[:1])
     fresh_sum.offer(0)
+    pl.when(core == 1)(down_sum[0].start)
+    down_sum[1].start()
     output(1, fresh_hidden, down_w, fresh, fresh_sum.order[1:2])
     fresh_sum.offer(1)
-    down_sum[1].start()
     output(1, fresh_hidden, down_w, fresh, fresh_sum.order[2:], 0, 2)
     fresh_sum.join(0)
     fresh_sum.ring.start()
@@ -414,15 +414,16 @@
     hidden(1, upstream, down_w, keep_back, 2, 4)
     grad(1, saved_t, pre_grad, grad_up)
     up_sum[1].start()
-    output(None, pre_grad, up_w, saved, saved_sum.order[:2])
-    saved_sum.offer(0, 1)
-    output(None, pre_grad, up_w, saved, saved_sum.order[2:], 0, 2)
+    output(None, pre_grad, up_w, saved, saved_sum.order[:1])
+    saved_sum.offer(0)
+    output(None, pre_grad, up_w, saved, saved_sum.order[1:2])
+    saved_sum.offer(1)
     saved_sum.join(0)
     saved_sum.ring.start()
+    up_sum[0].mid()
+    output(None, pre_grad, up_w, saved, saved_sum.order[2:])
+    saved_sum.offer(2, 3)
     saved_sum.join(1)
-    up_sum[0].mid()
-    output(None, pre_grad, up_w, saved, saved_sum.order[2:], 2, 4)
-    saved_sum.offer(2, 3)
     down_sum[0].turn()
     saved_sum.join(2)
     saved_sum.ring.rest()

time: 99.5 us -> 99.1 us (level)
  no operation moved by 1% of the time
where the time goes in v5:
time: 99.1 us; the launch traced here: 98.9 us
  Pallas kernels  98.1 us (99%)
    pallas_call x1, Pallas kernels, body(): pl.pallas_call(kernel, out_shape=(pltpu.VMEM((128, 2048), BF), pltpu.VMEM...  96.8 us

profile of v5, /device:TPU:1, one launch (start us, length us, event | category | flops | bytes accessed | tf_op | source)
XLA Modules:
  0.0 98.9 jit_solution(8932992506237325288)
XLA Ops:
  0.6 96.8 %shard_map.102 = (bf16[128,2048]{1,0:T(8,128)(2,1)S(1)}, bf16[128,2048]{1,0:T(8,128)(2,1)S(1)}, f32[128,1024]{1,0:T(8,128)S(1)}, f32[128,1024]{1,0:T(8,128)S(1)}) custom-call(bf16[4,256,2048]{2,1,0:T(8,128)(2,1)} %bitcast.3, bf16[4,256,2048]{2,1,0:T(8,128)(2,1)} %bitcast.4, bf16[4,256,2048]{2,1,0:T(8,128)(2,1)} %bitcast.5, bf16[128,1024]{1,0:T(8,128)(2,1)} %up_hbm.1, ...), custom_call_target="tpu_custom_call" | custom-call | flops 30064771072 | bytes 33554432 | tf_op jit(solution)/shard_map/pallas_call | solution.py:463
  97.4 1.3 %shard_map.103 = (bf16[128,2048]{1,0:T(8,128)(2,1)}, bf16[128,2048]{1,0:T(8,128)(2,1)}, f32[128,1024]{1,0:T(8,128)}, f32[128,1024]{1,0:T(8,128)}) custom-call(bf16[128,2048]{1,0:T(8,128)(2,1)S(1)} %get-tuple-element.8.refs_0_, bf16[128,2048]{1,0:T(8,128)(2,1)S(1)} %get-tuple-element.9.refs_1_, f32[128,1024]{1,0:T(8,128)S(1)} %get-tuple-element.10.refs_2_, ...), custom_call_target="tpu_custom_call" | custom-call | tf_op jit(solution)/shard_map/pallas_call | solution.py:506

commit v6 on v5

--- a/solution.py
+++ b/solution.py
@@ -60,22 +60,25 @@
         )
 
     class Ring:
-        def __init__(self, axis, pool):
+        def __init__(self, axis, pool, mate):
             self.plus, self.minus = to[(axis, 1)], to[(axis, -1)]
             p = place[axis]
             self.here, self.after, self.across, self.before = p, nxt(p, 1), nxt(p, 2), nxt(p, 3)
-            self.out, self.into = pool, reserve(3)
+            self.out, self.into = pool, reserve(2)
+            self.last = mate.last if mate else reserve(1)
 
         def push(self, src, dst, slot, target):
-            message(src, dst, self.out, self.into + slot, target).start()
+            where = self.last if slot == 2 else self.into + slot
+            message(src, dst, self.out, where, target).start()
 
         def got(self, dst, slot):
-            message(dst, dst, self.out, self.into + slot, self.plus).wait_recv()
+            where = self.last if slot == 2 else self.into + slot
+            message(dst, dst, self.out, where, self.plus).wait_recv()
 
     class Gather(Ring):
-        def __init__(self, axis, block, two, pool):
-            super().__init__(axis, pool)
-            self.block, self.two = block, two
+        def __init__(self, axis, block, landed, pool, mate=None):
+            super().__init__(axis, pool, mate)
+            self.block, self.landed = block, landed
 
         def go(self, half, slot, owner, target):
             part = self.block(owner, half)
@@ -96,12 +99,13 @@
             self.go(1, 2, self.after, self.minus)
 
         def end(self):
-            self.got(self.two, 2)
+            if self.landed is not None:
+                self.got(self.landed, 2)
 
     class Scatter(Ring):
-        def __init__(self, axis, block, land, pool):
-            super().__init__(axis, pool)
-            self.block, self.land = block, land
+        def __init__(self, axis, block, land, landed, pool, mate=None):
+            super().__init__(axis, pool, mate)
+            self.block, self.land, self.landed = block, land, landed
 
         def go(self, half, slot, index, owner, target):
             self.push(self.block(owner, half), self.land.at[index], slot, target)
@@ -127,7 +131,8 @@
             self.go(1, 2, 5, self.before, self.minus)
 
         def end(self, store):
-            self.got(self.land.at[pl.ds(2, 4)], 2)
+            if self.landed is not None:
+                self.got(self.landed, 2)
             for half, parts in ((0, (3, 4)), (1, (2, 5))):
                 total = self.block(self.here, half)[...].astype(F32)
                 for index in parts:
@@ -144,56 +149,44 @@
                     getattr(ring, step)()
             return run
 
-    def gather_1(w, cols, pool):
+    def gather_1(w, cols, landed, pool):
         a, b = cols
-        return Both(
-            Gather(
-                "y", lambda p, h: w.at[z, rows_at(p * 128 + h * 64, 64), a],
-                w.at[0, pl.ds(0, 256), a], pool,
-            ),
-            Gather(
-                "z", lambda p, h: w.at[p, rows_at(y * 128 + h * 64, 64), b],
-                w.at[0, pl.ds(0, 256), b], pool,
-            ),
+        one = Gather("y", lambda p, h: w.at[z, rows_at(p * 128 + h * 64, 64), a], landed, pool)
+        other = Gather(
+            "z", lambda p, h: w.at[p, rows_at(y * 128 + h * 64, 64), b], None, pool, one
         )
+        return Both(one, other)
 
     def gather_2(w, q, pool):
         a, b = GROUPS[q]
-        return Both(
-            Gather(
-                "z", lambda p, h: w.at[p, pl.ds(h * 256, 256), a],
-                w.at[pl.ds(0, 2), :, a], pool,
-            ),
-            Gather(
-                "y", lambda p, h: w.at[pl.ds(h * 2, 2), rows_at(p * 128, 128), b],
-                w.at[:, pl.ds(0, 256), b], pool,
-            ),
+        one = Gather("z", lambda p, h: w.at[p, pl.ds(h * 256, 256), a], w.at[0], pool)
+        other = Gather(
+            "y", lambda p, h: w.at[pl.ds(h * 2, 2), rows_at(p * 128, 128), b], None, pool, one
         )
+        return Both(one, other)
 
     class GradSum:
         def __init__(self, grad, which, q, accum, out):
             a, b = GROUPS[q]
             self.q, self.accum, self.out = q, accum, out
-            self.one = (
-                Scatter(
-                    "z", lambda p, h: grad.at[p, pl.ds(h * 256, 256), a],
-                    land_z.at[which, q], 2,
-                ),
-                Scatter(
-                    "y", lambda p, h: grad.at[pl.ds(h * 2, 2), rows_at(p * 128, 128), b],
-                    land_y.at[which, q], 3,
-                ),
-            )
-            self.two = (
-                Scatter(
-                    "y", lambda p, h: grad.at[z, rows_at(p * 128 + h * 64, 64), a],
-                    land_2.at[which, q, 0], 4,
-                ),
-                Scatter(
-                    "z", lambda p, h: grad.at[p, rows_at(y * 128 + h * 64, 64), b],
-                    land_2.at[which, q, 1], 4,
-                ),
-            )
+            one = Scatter(
+                "z", lambda p, h: grad.at[p, pl.ds(h * 256, 256), a],
+                land_z.at[which, q], grad.at[0], 2,
+            )
+            other = Scatter(
+                "y", lambda p, h: grad.at[pl.ds(h * 2, 2), rows_at(p * 128, 128), b],
+                land_y.at[which, q], None, 3, one,
+            )
+            self.one = (one, other)
+            one = Scatter(
+                "y", lambda p, h: grad.at[z, rows_at(p * 128 + h * 64, 64), a],
+                land_2.at[which, q, 0], grad.at[0, pl.ds(0, 128)], 4,
+            )
+            other = Scatter(
+                "z", lambda p, h: grad.at[p, rows_at(y * 128 + h * 64, 64), b],
+                land_2.at[which, q, 1], None, 4, one,
+            )
+            self.two = (one, other)
 
         def start(self):
             for ring in self.one:
@@ -231,7 +224,7 @@
             self.order = (nxt(x, 2), nxt(x, 1), nxt(x, 3), x)
             self.ring = Scatter(
                 "x", lambda p, h: part.at[p, rows_at(core * 128 + h * 64, 64), :],
-                land_x.at[which], 5,
+                land_x.at[which], land_x.at[which, pl.ds(2, 4)], 5,
             )
 
         def pair(self, src, step):
@@ -273,8 +266,8 @@
         pl.semaphore_signal(barrier, inc=1, device_id=target, device_id_type=MESH)
     pl.semaphore_wait(barrier, len(to))
 
-    up_1 = [gather_1(up_w, cols, 0) for cols in GROUPS]
-    up_2, down_1 = (gather_2(up_w, 0, 0), gather_2(up_w, 1, 0)), gather_1(down_w, COLS, 1)
+    up_1 = [gather_1(up_w, cols, up_w.at[0, pl.ds(0, 128)], 0) for cols in GROUPS]
+    up_2, down_1 = (gather_2(up_w, 0, 0), gather_2(up_w, 1, 0)), gather_1(down_w, COLS, down_w.at[0, pl.ds(0, 256)], 1)
     down_2 = (gather_2(down_w, 0, 1), gather_2(down_w, 1, 1))
     grad_up = upstream_t
     down_sum = [GradSum(grad_down, 0, q, accum_down, accum_down_out) for q in range(2)]
@@ -391,10 +384,10 @@
 
     output(1, fresh_hidden, down_w, fresh, fresh_sum.order[:1])
     fresh_sum.offer(0)
+    output(1, fresh_hidden, down_w, fresh, fresh_sum.order[1:2])
+    fresh_sum.offer(1)
     pl.when(core == 1)(down_sum[0].start)
     down_sum[1].start()
-    output(1, fresh_hidden, down_w, fresh, fresh_sum.order[1:2])
-    fresh_sum.offer(1)
     output(1, fresh_hidden, down_w, fresh, fresh_sum.order[2:], 0, 2)
     fresh_sum.join(0)
     fresh_sum.ring.start()
@@ -489,7 +482,7 @@
             pltpu.VMEM((2, 4, 128, 2048), BF),
             pltpu.VMEM((2, 6, 64, 2048), BF),
             pltpu.SemaphoreType.DMA((7,)),
-            pltpu.SemaphoreType.DMA((N_RINGS * 3 + 8,)),
+            pltpu.SemaphoreType.DMA((N_RINGS * 3 - 15 + 8,)),
             pltpu.SemaphoreType.DMA((7,)),
         ],
         compiler_params=pltpu.CompilerParams(

time: 99.1 us -> 98.9 us (level)
  no operation moved by 1% of the time
where the time goes in v6:
time: 98.9 us; the launch traced here: 98.8 us
  Pallas kernels  98 us (99%)
    pallas_call x1, Pallas kernels, body(): pl.pallas_call(kernel, out_shape=(pltpu.VMEM((128, 2048), BF), pltpu.VMEM...  96.6 us

profile of v6, /device:TPU:1, one launch (start us, length us, event | category | flops | bytes accessed | tf_op | source)
XLA Modules:
  0.0 98.8 jit_solution(8041126404396627057)
XLA Ops:
  0.6 96.6 %shard_map.102 = (bf16[128,2048]{1,0:T(8,128)(2,1)S(1)}, bf16[128,2048]{1,0:T(8,128)(2,1)S(1)}, f32[128,1024]{1,0:T(8,128)S(1)}, f32[128,1024]{1,0:T(8,128)S(1)}) custom-call(bf16[4,256,2048]{2,1,0:T(8,128)(2,1)} %bitcast.3, bf16[4,256,2048]{2,1,0:T(8,128)(2,1)} %bitcast.4, bf16[4,256,2048]{2,1,0:T(8,128)(2,1)} %bitcast.5, bf16[128,1024]{1,0:T(8,128)(2,1)} %up_hbm.1, ...), custom_call_target="tpu_custom_call" | custom-call | flops 30064771072 | bytes 33554432 | tf_op jit(solution)/shard_map/pallas_call | solution.py:456
  97.3 1.3 %shard_map.103 = (bf16[128,2048]{1,0:T(8,128)(2,1)}, bf16[128,2048]{1,0:T(8,128)(2,1)}, f32[128,1024]{1,0:T(8,128)}, f32[128,1024]{1,0:T(8,128)}) custom-call(bf16[128,2048]{1,0:T(8,128)(2,1)S(1)} %get-tuple-element.8.refs_0_, bf16[128,2048]{1,0:T(8,128)(2,1)S(1)} %get-tuple-element.9.refs_1_, f32[128,1024]{1,0:T(8,128)S(1)} %get-tuple-element.10.refs_2_, ...), custom_call_target="tpu_custom_call" | custom-call | tf_op jit(solution)/shard_map/pallas_call | solution.py:499

commit v7 on v6

--- a/solution.py
+++ b/solution.py
@@ -381,13 +381,14 @@
     output(0, fresh_hidden, down_w, fresh, fresh_sum.order[2:])
     pl.when(core == 0)(down_sum[0].start)
     down_2[1].end()
+    pl.when(core == 0)(down_sum[1].start)
 
     output(1, fresh_hidden, down_w, fresh, fresh_sum.order[:1])
     fresh_sum.offer(0)
     output(1, fresh_hidden, down_w, fresh, fresh_sum.order[1:2])
     fresh_sum.offer(1)
     pl.when(core == 1)(down_sum[0].start)
-    down_sum[1].start()
+    pl.when(core == 1)(down_sum[1].start)
     output(1, fresh_hidden, down_w, fresh, fresh_sum.order[2:], 0, 2)
     fresh_sum.join(0)
     fresh_sum.ring.start()

time: 98.9 us -> 98.9 us (level)
  no operation moved by 1% of the time
where the time goes in v7:
time: 98.9 us; the launch traced here: 98.8 us
  Pallas kernels  98 us (99%)
    pallas_call x1, Pallas kernels, body(): pl.pallas_call(kernel, out_shape=(pltpu.VMEM((128, 2048), BF), pltpu.VMEM...  96.6 us

profile of v7, /device:TPU:1, one launch (start us, length us, event | category | flops | bytes accessed | tf_op | source)
XLA Modules:
  0.0 98.8 jit_solution(8170928996758416361)
XLA Ops:
  0.6 96.6 %shard_map.102 = (bf16[128,2048]{1,0:T(8,128)(2,1)S(1)}, bf16[128,2048]{1,0:T(8,128)(2,1)S(1)}, f32[128,1024]{1,0:T(8,128)S(1)}, f32[128,1024]{1,0:T(8,128)S(1)}) custom-call(bf16[4,256,2048]{2,1,0:T(8,128)(2,1)} %bitcast.3, bf16[4,256,2048]{2,1,0:T(8,128)(2,1)} %bitcast.4, bf16[4,256,2048]{2,1,0:T(8,128)(2,1)} %bitcast.5, bf16[128,1024]{1,0:T(8,128)(2,1)} %up_hbm.1, ...), custom_call_target="tpu_custom_call" | custom-call | flops 30064771072 | bytes 33554432 | tf_op jit(solution)/shard_map/pallas_call | solution.py:457
  97.2 1.3 %shard_map.103 = (bf16[128,2048]{1,0:T(8,128)(2,1)}, bf16[128,2048]{1,0:T(8,128)(2,1)}, f32[128,1024]{1,0:T(8,128)}, f32[128,1024]{1,0:T(8,128)}) custom-call(bf16[128,2048]{1,0:T(8,128)(2,1)S(1)} %get-tuple-element.8.refs_0_, bf16[128,2048]{1,0:T(8,128)(2,1)S(1)} %get-tuple-element.9.refs_1_, f32[128,1024]{1,0:T(8,128)S(1)} %get-tuple-element.10.refs_2_, ...), custom_call_target="tpu_custom_call" | custom-call | tf_op jit(solution)/shard_map/pallas_call | solution.py:500
